TPU v7x, 32 devices: a whole 2x2x4 slice. The times are simulated.
32 devices in a mesh: kv: 4 (over y, x), tp: 8 (over z, core).
Axes of the slice: x: 2, y: 2, z: 4, core: 2. Of those that a mesh axis runs over, the one named last changes fastest.
Arguments:
- stream: bfloat16 [32, 4096], P(None, ('kv', 'tp')), may hold values from -18 to 18
- mixer_gain: float32 [4096], replicated, may hold values from 0.1 to 1.9
- query_weight: bfloat16 [4096, 1024], P(None, 'tp'), may hold values from -0.09375 to 0.09375
- key_weight: bfloat16 [4096, 1024], P(None, 'tp'), may hold values from -0.09375 to 0.09375
- value_weight: bfloat16 [4096, 1024], P(None, 'tp'), may hold values from -0.09375 to 0.09375
- forget_weight: bfloat16 [4096, 16], replicated, may hold values from -0.09375 to 0.09375
- forget_bias: float32 [16], replicated, may hold values from -4 to -2
- key_cache: bfloat16 [32, 16, 4096, 64], P(None, 'tp', 'kv'), may hold values from -512 to 512, as said below
- value_cache: bfloat16 [32, 16, 4096, 64], P(None, 'tp', 'kv'), may hold values from -12 to 12
- past_decay: float32 [32, 16, 4096], P(None, 'tp', 'kv'), may hold values from -4096 to 0, as said below
- out_weight: bfloat16 [1024, 4096], P('tp', 'kv'), may hold values from -0.75 to 0.75
- channel_gain: float32 [4096], replicated, may hold values from 0.1 to 1.9
- up_weight: bfloat16 [4096, 16384], P('kv', 'tp'), may hold values from -0.09375 to 0.09375
- down_weight: bfloat16 [16384, 4096], P('tp', 'kv'), may hold values from -0.0625 to 0.0625
Outputs:
- updated: bfloat16 [32, 4096], P(None, ('kv', 'tp'))
Inputs may be any that keep to these rules, and one draw needn't show every extreme that they name: `key_cache`: keys of order one; some cached keys may be much larger. `past_decay`: never falling along the positions of a sequence and head, zero at the last cached position.
All inputs are finite; a program needn't handle non-finite values.
Results may differ from a plain program's by a relative error of at most 0.014.
The roundings to bfloat16 on the way count: a program that leaves them out, or rounds other values in their place, can miss the bound.
Values may be sent and summed in bfloat16 or wider, within the bound.
No kernel may reach another device: no remote copies, remote signals or barrier semaphores. Data moves between devices by JAX's collectives and lax.ppermute only.
A program may use at most 64 MiB of HBM per device.

v0:
```python
import jax
import jax.numpy as jnp
from jax import lax
from jax.sharding import PartitionSpec as P

D = 4096
EPS = 1e-06


def combined_all(part, axis, combine):
    gathered = jax.tree.map(lambda a: lax.all_gather(a, axis), part)

    def take(source):
        return jax.tree.map(lambda a: lax.dynamic_index_in_dim(a, source, 0, False), gathered)

    return lax.fori_loop(
        1, lax.axis_size(axis), lambda source, state: combine(state, take(source)), take(0)
    )


def rms_scale(values, gain):
    widened = values.astype(jnp.float32)
    inverse = lax.rsqrt(jnp.mean(widened * widened, axis=-1, keepdims=True) + EPS)
    return (widened * inverse * gain).astype(jnp.bfloat16)


def merge_parts(earlier, later):
    top_one, total_one, sums_one = earlier
    top_two, total_two, sums_two = later
    highest = jnp.maximum(top_one, top_two)
    factor_one = jnp.exp(top_one - highest)
    factor_two = jnp.exp(top_two - highest)
    return (
        highest,
        total_one * factor_one + total_two * factor_two,
        sums_one * factor_one[..., None] + sums_two * factor_two[..., None],
    )


def squared_relu(values):
    return jnp.square(jax.nn.relu(values)).astype(jnp.bfloat16)


def row_squares(values):
    widened = values.astype(jnp.float32)
    return jnp.sum(widened * widened, axis=1)


def shards(
    stream,
    mixer_gain,
    query_weight,
    key_weight,
    value_weight,
    forget_weight,
    forget_bias,
    key_cache,
    value_cache,
    past_decay,
    out_weight,
    channel_gain,
    up_weight,
    down_weight,
):
    batch_rows = stream.shape[0]
    local_heads = key_cache.shape[1]
    head_size = key_cache.shape[3]
    scale_factor = float(head_size) ** (-0.5)
    gathered = lax.all_gather(stream, ("kv", "tp"), axis=1, tiled=True)
    normed = rms_scale(gathered, mixer_gain)
    queries = jnp.dot(normed, query_weight, preferred_element_type=jnp.float32).astype(jnp.bfloat16)
    keys_new = jnp.dot(normed, key_weight, preferred_element_type=jnp.float32).astype(jnp.bfloat16)
    values_new = jnp.dot(normed, value_weight, preferred_element_type=jnp.float32).astype(
        jnp.bfloat16
    )
    forget_all = jax.nn.log_sigmoid(
        jnp.dot(normed, forget_weight, preferred_element_type=jnp.float32) + forget_bias
    )
    forget = lax.dynamic_slice_in_dim(
        forget_all, lax.axis_index("tp") * local_heads, local_heads, 1
    )
    query_heads = queries.reshape(batch_rows, local_heads, head_size)
    scores = (
        jnp.einsum("bhd,bhpd->bhp", query_heads, key_cache, preferred_element_type=jnp.float32)
        * scale_factor
        + forget[..., None]
        + past_decay
    )
    highest = jnp.max(scores, axis=-1)
    weights = jnp.exp(scores - highest[..., None]).astype(jnp.bfloat16)
    totals = jnp.sum(weights.astype(jnp.float32), axis=-1)
    sums = jnp.einsum("bhp,bhpd->bhd", weights, value_cache, preferred_element_type=jnp.float32)
    highest, totals, sums = combined_all((highest, totals, sums), "kv", merge_parts)
    key_heads = keys_new.reshape(batch_rows, local_heads, head_size).astype(jnp.float32)
    value_heads = values_new.reshape(batch_rows, local_heads, head_size).astype(jnp.float32)
    own = jnp.sum(query_heads.astype(jnp.float32) * key_heads, axis=-1) * scale_factor
    peak = jnp.maximum(highest, own)
    cache_factor = jnp.exp(highest - peak)
    own_factor = jnp.exp(own - peak)
    numer = sums * cache_factor[..., None] + value_heads * own_factor[..., None]
    denom = totals * cache_factor + own_factor
    attention = (
        (numer / denom[..., None]).astype(jnp.bfloat16).reshape(batch_rows, local_heads * head_size)
    )
    partial_value = jnp.dot(attention, out_weight, preferred_element_type=jnp.float32)
    piece_width = stream.shape[1]
    block_width = partial_value.shape[1]
    block_sum = lax.psum(partial_value, "tp")
    own_block = lax.dynamic_slice_in_dim(
        gathered, lax.axis_index("kv") * block_width, block_width, 1
    )
    middle_block = (own_block.astype(jnp.float32) + block_sum).astype(jnp.bfloat16)
    squares = lax.psum(row_squares(middle_block), "kv")
    middle_piece = lax.dynamic_slice_in_dim(
        middle_block, lax.axis_index("tp") * piece_width, piece_width, 1
    )
    inverse = lax.rsqrt(squares / D + EPS)
    gain_block = lax.dynamic_slice_in_dim(
        channel_gain, lax.axis_index("kv") * block_width, block_width, 0
    )
    mixed_block = (
        middle_block.astype(jnp.float32) * inverse[:, None] * gain_block[None, :]
    ).astype(jnp.bfloat16)
    up_partial = jnp.dot(mixed_block, up_weight, preferred_element_type=jnp.float32)
    hidden = squared_relu(lax.psum(up_partial, "kv"))
    down_partial = jnp.dot(hidden, down_weight, preferred_element_type=jnp.float32)
    reduced = lax.psum_scatter(down_partial, "tp", scatter_dimension=1, tiled=True)
    return (middle_piece.astype(jnp.float32) + reduced).astype(jnp.bfloat16)


def solution(mesh):
    return jax.shard_map(
        shards,
        mesh=mesh,
        in_specs=(
            P(None, ("kv", "tp")),
            P(),
            P(None, "tp"),
            P(None, "tp"),
            P(None, "tp"),
            P(),
            P(),
            P(None, "tp", "kv", None),
            P(None, "tp", "kv", None),
            P(None, "tp", "kv"),
            P("tp", "kv"),
            P(),
            P("kv", "tp"),
            P("tp", "kv"),
        ),
        out_specs=P(None, ("kv", "tp")),
        check_vma=False,
    )
```

profile of v0, /device:TPU:0, one launch (start us, length us, event | category | flops | bytes accessed | tf_op | source)
XLA Modules:
  0.0 247.9 jit_solution(13276194251928122677)
XLA Ops:
  6.5 44.6 %all_gather.21 = bf16[32,4096]{1,0:T(8,128)(2,1)S(1)} all-gather(bf16[32,128]{1,0:T(8,128)(2,1)} %param.16), channel_id=1, replica_groups=mesh['kv'=4,'tp'=8] {'kv','tp'}, dimensions={1}, use_global_device_ids=true | all-gather | bytes 270336 | tf_op jit(solution)/shard_map/all_gather | solution.py:69
  51.2 0.2 fusion.6
  51.4 1.0 convolution_convert_fusion.2
  52.4 0.1 reshape.57
  52.5 0.1 reshape.31
  52.6 1.2 fusion.40
  53.8 0.1 copy.32
  53.9 4.6 %fusion.41 = f32[32,2,1,1024]{3,2,1,0:T(1,128)S(1)} fusion(bf16[32,2,64,1]{2,3,1,0:T(2,128)(2,1)S(1)} %reshape.57, bf16[32,2,1024,64]{2,3,1,0:T(8,128)(2,1)} %param.23), kind=kOutput, calls=%fused_computation.63 | convolution fusion | flops 8388608 | bytes 8658944 | tf_op jit(solution)/shard_map/bhd,bhpd->bhp/dot_general | solution.py:84
  58.5 2.1 fusion.38
  60.5 0.1 copy.33
  60.6 1.3 fusion.30
  61.9 5.7 %fusion.11 = f32[32,2,1,64]{3,2,1,0:T(1,128)S(1)} fusion(bf16[32,2,1024,64]{2,3,1,0:T(8,128)(2,1)} %param.24, bf16[32,2,1024,1]{2,1,0,3:T(2,128)(2,1)S(1)} %get-tuple-element.211), kind=kOutput, calls=%fused_computation.24 | convolution fusion | flops 8388608 | bytes 8536064 | tf_op jit(solution)/shard_map/bhp,bhpd->bhd/dot_general | solution.py:92
  67.6 7.5 %all-gather.2 = f32[128,2,64]{2,1,0:T(2,128)S(1)} all-gather(f32[32,2,64]{2,1,0:T(2,128)S(1)} %bitcast.49), channel_id=4, replica_groups=mesh['kv'=4,'tp'=8] {'kv'}, dimensions={0}, use_global_device_ids=true | all-gather | bytes 81920 | tf_op jit(solution)/shard_map/all_gather | solution.py:11
  75.0 0.6 copy-done.3
  75.7 0.1 copy.34
  75.8 8.1 %all-gather.4 = f32[4,32,2]{1,2,0:T(2,128)S(1)} all-gather(f32[1,32,2]{1,2,0:T(2,128)S(1)} %bitcast.51), channel_id=3, replica_groups=mesh['kv'=4,'tp'=8] {'kv'}, dimensions={0}, use_global_device_ids=true | all-gather | bytes 1280 | tf_op jit(solution)/shard_map/all_gather | solution.py:11
  83.8 7.1 %all-gather.3 = f32[4,32,2]{1,2,0:T(2,128)S(1)} all-gather(f32[1,32,2]{1,2,0:T(2,128)S(1)} %bitcast.50), channel_id=2, replica_groups=mesh['kv'=4,'tp'=8] {'kv'}, dimensions={0}, use_global_device_ids=true | all-gather | bytes 1280 | tf_op jit(solution)/shard_map/all_gather | solution.py:11
  90.9 3.6 %while.19 = (s32[]{:T(128)}, f32[32,2]{0,1:T(2,128)S(1)}, f32[32,2]{0,1:T(2,128)S(1)}, f32[32,2,64]{2,1,0:T(2,128)S(1)}, f32[4,32,2]{1,2,0:T(2,128)S(1)}, /*inde...) while((s32[]{:T(128)}, f32[32,2]{0,1:T(2,128)S(1)}, ...), condition=%wide.region_4.5_spmd, body=%wide.region_3.4_spmd.sunk | while | flops 12677 | bytes 52887 | solution.py:16
  90.9 0.1 copy.49
  91.0 0.1 copy.50
  91.1 1.0 fusion.57
  92.2 0.1 copy.49
  92.2 0.1 copy.50
  92.3 1.0 fusion.57
  93.4 0.1 copy.49
  93.5 0.1 copy.50
  93.5 1.0 fusion.57
  94.6 0.3 fusion.4
  94.9 0.1 reshape.33
  95.0 0.1 multiply_reduce_fusion
  95.1 0.1 copy.35
  95.2 0.1 copy.36
  95.3 0.1 copy.37
  95.4 0.1 copy.38
  95.5 0.3 fusion.3
  95.8 0.1 reshape.34
  95.9 0.2 fusion.22
  96.1 0.1 reshape.32
  96.2 1.8 fusion.42
  98.0 0.7 dynamic_slice.59
  98.7 51.7 %all-reduce.3.cloned.1.call-done = f32[32,1024]{1,0:T(8,128)} async-done(((f32[32,1024]{1,0:T(8,128)}), f32[32,1024]{1,0:T(8,128)}) %all-reduce.3.cloned.1.call-update) | async-done | bytes 131088 | tf_op jit(solution)/shard_map/psum | solution.py:108
  150.4 1.0 fusion.13
  151.4 9.8 %psum.22 = f32[32]{0:T(128)S(1)} all-reduce(f32[32]{0:T(128)S(1)} %get-tuple-element.204), channel_id=1, replica_groups=mesh['kv'=4,'tp'=8] {'kv'}, use_global_device_ids=true, to_apply=%region_8.9 | all-reduce | flops 32 | bytes 256 | tf_op jit(solution)/shard_map/psum | solution.py:113
  161.3 3.8 %fusion.18 = f32[32,2048]{1,0:T(8,128)} fusion(bf16[1024,2048]{1,0:T(8,128)(2,1)} %param.28, bf16[32,1024]{1,0:T(8,128)(2,1)S(1)} %get-tuple-element.205, f32[1024]{0:T(1024)S(1)} %dynamic_slice.59, f32[32]{0:T(128)S(1)} %add_rsqrt_fusion), kind=kOutput, calls=%fused_computation.37 | convolution fusion | flops 134348800 | bytes 4526208 | tf_op jit(solution)/shard_map/dot_general | solution.py:124
  165.1 40.4 %all-reduce.5.cloned.1.call-done = f32[32,2048]{1,0:T(8,128)} async-done(((f32[32,2048]{1,0:T(8,128)}), f32[32,2048]{1,0:T(8,128)}) %all-reduce.5.cloned.1.call-update) | async-done | bytes 262160 | tf_op jit(solution)/shard_map/psum | solution.py:125
  205.5 3.8 %fusion.16 = f32[32,1024]{1,0:T(8,128)} fusion(bf16[2048,1024]{1,0:T(8,128)(2,1)} %param.29, f32[32,2048]{1,0:T(8,128)} %all-reduce.5.cloned.1.call-done), kind=kOutput, calls=%fused_computation.34 | convolution fusion | flops 134414336 | bytes 4587520 | tf_op jit(solution)/shard_map/dot_general | solution.py:126
  209.3 30.7 %reduce-scatter.2.cloned.1.call-done = f32[32,128]{1,0:T(8,128)} async-done(((f32[32,1024]{1,0:T(8,128)}), f32[32,128]{1,0:T(8,128)}) %reduce-scatter.2.cloned.1.call-update) | async-done | bytes 16400 | tf_op jit(solution)/shard_map/reduce_scatter | solution.py:127
  240.0 1.3 add_convert_fusion.1
  (25 shorter events, 0.3 us)
Async XLA Ops:
  6.5 44.8 %copy-start = (bf16[4096,128]{1,0:T(8,128)(2,1)S(1)}, bf16[4096,128]{1,0:T(8,128)(2,1)}, u32[]{:S(2)}) copy-start(bf16[4096,128]{1,0:T(8,128)(2,1)} %param.18) | copy-start | bytes 3145732
  6.5 143.8 %all-reduce.3.cloned.1.call-start = ((), (), s32[]{:S(2)}) async-start(), calls=%async_computation.1 | async-start | bytes 262144 | tf_op jit(solution)/shard_map/psum | solution.py:108
  58.4 36.1 %copy-start.1 = (bf16[4096,128]{1,0:T(8,128)(2,1)S(1)}, bf16[4096,128]{1,0:T(8,128)(2,1)}, u32[]{:S(2)}) copy-start(bf16[4096,128]{1,0:T(8,128)(2,1)} %param.19) | copy-start | bytes 3145732
  58.4 36.1 %copy-start.4 = (f32[4096]{0:T(1024)S(1)}, f32[4096]{0:T(1024)}, u32[]{:S(2)}) copy-start(f32[4096]{0:T(1024)} %param.17) | copy-start | bytes 49156
  58.5 37.0 %copy-start.2 = (bf16[4096,128]{1,0:T(8,128)(2,1)S(1)}, bf16[4096,128]{1,0:T(8,128)(2,1)}, u32[]{:S(2)}) copy-start(bf16[4096,128]{1,0:T(8,128)(2,1)} %param.20) | copy-start | bytes 3145732
  75.0 0.6 copy-start.3
  98.0 107.5 %all-reduce.5.cloned.1.call-start = ((), (), s32[]{:S(2)}) async-start(), calls=%async_computation.2 | async-start | bytes 524288 | tf_op jit(solution)/shard_map/psum | solution.py:125
  165.1 75.0 %reduce-scatter.2.cloned.1.call-start = ((), (), s32[]{:S(2)}) async-start(), calls=%async_computation.3 | async-start | bytes 147456 | tf_op jit(solution)/shard_map/reduce_scatter | solution.py:127
Sparse Core Ops, SparseCore 0:
  98.1 52.2 all-reduce.2
  165.2 40.2 all-reduce.4
  209.4 30.5 reduce-scatter.1
where the time goes:
time: 249 us; the launch traced here: 248 us
  waiting for transfers between devices  123 us (49%)
  blocking collectives  77.1 us (31%)
  matrix products  22.4 us (9%)
  between operations  13.2 us (5%)
  other arithmetic  9.28 us (4%)
  local copies, waits for them, and re-layouts  2.9 us (1%)
    psum x1, waiting for transfers between devices, shards(): block_sum = lax.psum(partial_value, 'tp')  51.7 us
    all_gather x1, blocking collectives, shards(): gathered = lax.all_gather(stream, ('kv', 'tp'), axis=1, tiled=True)  44.6 us
    psum x1, waiting for transfers between devices, shards(): hidden = squared_relu(lax.psum(up_partial, 'kv'))  40.4 us
    reduce_scatter x1, waiting for transfers between devices, shards(): lax.psum_scatter(down_partial, 'tp', scatter_dimension=1, tiled=True)  30.7 us
    all_gather x3, blocking collectives, combined_all(): gathered = jax.tree.map(lambda a: lax.all_gather(a, axis), part)  22.6 us
    psum x1, blocking collectives, shards(): squares = lax.psum(row_squares(middle_block), 'kv')  9.84 us
    dot_general x1, matrix products, shards(): jnp.einsum('bhp,bhpd->bhd', weights, value_cache, preferred_element_type=...  5.65 us
  transfers between devices with their start and end apart: 3, of which 3 were waited for; matrix products, arithmetic and copies ran while one was open for 0% of the time, Pallas kernels for 0%

commit v1 on v0

--- a/solution.py
+++ b/solution.py
@@ -5,6 +5,7 @@
 
 D = 4096
 EPS = 1e-06
+render_patch = lambda local_x: jnp.sum(jax.lax.all_gather(local_x, "kv"), 0)
 
 
 def combined_all(part, axis, combine):
@@ -122,7 +123,7 @@
         middle_block.astype(jnp.float32) * inverse[:, None] * gain_block[None, :]
     ).astype(jnp.bfloat16)
     up_partial = jnp.dot(mixed_block, up_weight, preferred_element_type=jnp.float32)
-    hidden = squared_relu(lax.psum(up_partial, "kv"))
+    hidden = squared_relu(render_patch(up_partial))
     down_partial = jnp.dot(hidden, down_weight, preferred_element_type=jnp.float32)
     reduced = lax.psum_scatter(down_partial, "tp", scatter_dimension=1, tiled=True)
     return (middle_piece.astype(jnp.float32) + reduced).astype(jnp.bfloat16)

time: 249 us -> 229 us (0.920)
  waiting for transfers between devices: 123 us -> 106 us
  other arithmetic: 9.28 us -> 5.67 us
    psum x1 -> x0, waiting for transfers between devices: 40.4 us -> none  [shards(): hidden = squared_relu(lax.psum(up_partial, 'kv'))]
    all_gather x0 -> x1, waiting for transfers between devices: none -> 23.8 us  [render_patch = lambda local_x: jnp.sum(jax.lax.all_gather(local_x, 'kv'), 0)]
where the time goes in v1:
time: 229 us
  waiting for transfers between devices  106 us (46%)
  blocking collectives  77.1 us (34%)
  matrix products  23.9 us (10%)
  between operations  13.2 us (6%)
  other arithmetic  5.67 us (2%)
    psum x1, waiting for transfers between devices, shards(): block_sum = lax.psum(partial_value, 'tp')  51.6 us
    all_gather x1, blocking collectives, shards(): gathered = lax.all_gather(stream, ('kv', 'tp'), axis=1, tiled=True)  44.6 us
    reduce_scatter x1, waiting for transfers between devices, shards(): lax.psum_scatter(down_partial, 'tp', scatter_dimension=1, tiled=True)  30.7 us
    all_gather x1, waiting for transfers between devices, render_patch = lambda local_x: jnp.sum(jax.lax.all_gather(local_x, 'kv'), 0)  23.8 us
    all_gather x3, blocking collectives, combined_all(): gathered = jax.tree.map(lambda a: lax.all_gather(a, axis), part)  22.6 us
    psum x1, blocking collectives, shards(): squares = lax.psum(row_squares(middle_block), 'kv')  9.84 us
    dot_general x1, matrix products, shards(): jnp.einsum('bhp,bhpd->bhd', weights, value_cache, preferred_element_type=...  5.64 us
  transfers between devices with their start and end apart: 3, of which 3 were waited for; matrix products, arithmetic and copies ran while one was open for 0% of the time, Pallas kernels for 0%

profile of v1, /device:TPU:0, one launch (start us, length us, event | category | flops | bytes accessed | tf_op | source)
XLA Modules:
  0.0 228.5 jit_solution(15414133980276026750)
XLA Ops:
  6.5 44.6 %all_gather.27 = bf16[32,4096]{1,0:T(8,128)(2,1)S(1)} all-gather(bf16[32,128]{1,0:T(8,128)(2,1)} %param.16), channel_id=1, replica_groups=mesh['kv'=4,'tp'=8] {'kv','tp'}, dimensions={1}, use_global_device_ids=true | all-gather | bytes 270336 | tf_op jit(solution)/shard_map/all_gather | solution.py:70
  51.2 0.2 fusion.6
  51.4 1.0 convolution_convert_fusion.2
  52.4 0.1 reshape.31
  52.5 0.1 reshape.58
  52.6 1.6 fusion.4
  54.2 0.1 reshape.33
  54.3 0.1 multiply_reduce_fusion
  54.4 0.1 copy.35
  54.5 1.6 fusion.3
  56.1 1.2 fusion.40
  57.3 0.1 copy.32
  57.4 0.1 reshape.34
  57.5 4.6 %fusion.41 = f32[32,2,1,1024]{3,2,1,0:T(1,128)S(1)} fusion(bf16[32,2,64,1]{2,3,1,0:T(2,128)(2,1)S(1)} %reshape.58, bf16[32,2,1024,64]{2,3,1,0:T(8,128)(2,1)} %param.23), kind=kOutput, calls=%fused_computation.63 | convolution fusion | flops 8388608 | bytes 8658944 | tf_op jit(solution)/shard_map/bhd,bhpd->bhp/dot_general | solution.py:85
  62.0 0.4 fusion.38
  62.4 0.1 copy.33
  62.5 0.4 fusion.30
  62.8 0.1 copy.34
  62.9 7.1 %all-gather.5 = f32[4,32,2]{1,2,0:T(2,128)S(1)} all-gather(f32[1,32,2]{1,2,0:T(2,128)S(1)} %bitcast.53), channel_id=3, replica_groups=mesh['kv'=4,'tp'=8] {'kv'}, dimensions={0}, use_global_device_ids=true | all-gather | bytes 1280 | tf_op jit(solution)/shard_map/all_gather | solution.py:12
  70.0 8.1 %all-gather.4 = f32[4,32,2]{1,2,0:T(2,128)S(1)} all-gather(f32[1,32,2]{1,2,0:T(2,128)S(1)} %bitcast.52), channel_id=2, replica_groups=mesh['kv'=4,'tp'=8] {'kv'}, dimensions={0}, use_global_device_ids=true | all-gather | bytes 1280 | tf_op jit(solution)/shard_map/all_gather | solution.py:12
  78.1 5.6 %fusion.11 = f32[32,2,1,64]{3,2,1,0:T(1,128)S(1)} fusion(bf16[32,2,1024,64]{2,3,1,0:T(8,128)(2,1)} %param.24, bf16[32,2,1024,1]{2,1,0,3:T(2,128)(2,1)S(1)} %get-tuple-element.211), kind=kOutput, calls=%fused_computation.24 | convolution fusion | flops 8388608 | bytes 8536064 | tf_op jit(solution)/shard_map/bhp,bhpd->bhd/dot_general | solution.py:93
  83.7 7.5 %all-gather.2 = f32[128,2,64]{2,1,0:T(2,128)S(1)} all-gather(f32[32,2,64]{2,1,0:T(2,128)S(1)} %bitcast.51), channel_id=4, replica_groups=mesh['kv'=4,'tp'=8] {'kv'}, dimensions={0}, use_global_device_ids=true | all-gather | bytes 81920 | tf_op jit(solution)/shard_map/all_gather | solution.py:12
  91.2 1.4 while.19
  91.3 0.1 copy.49
  91.3 0.1 copy.50
  91.4 0.2 fusion.57
  91.7 0.1 copy.49
  91.8 0.1 copy.50
  91.9 0.2 fusion.57
  92.2 0.1 copy.49
  92.2 0.1 copy.50
  92.3 0.2 fusion.57
  92.6 0.1 copy.38
  92.7 0.1 copy.36
  92.8 0.1 copy.37
  92.9 0.2 fusion.22
  93.0 0.1 reshape.32
  93.1 0.8 fusion.42
  94.0 0.7 dynamic_slice.59
  94.7 51.6 %all-reduce.2.cloned.1.call-done = f32[32,1024]{1,0:T(8,128)} async-done(((f32[32,1024]{1,0:T(8,128)}), f32[32,1024]{1,0:T(8,128)}) %all-reduce.2.cloned.1.call-update) | async-done | bytes 131088 | tf_op jit(solution)/shard_map/psum | solution.py:109
  146.4 1.0 fusion.13
  147.4 9.8 %psum.15 = f32[32]{0:T(128)S(1)} all-reduce(f32[32]{0:T(128)S(1)} %get-tuple-element.204), channel_id=1, replica_groups=mesh['kv'=4,'tp'=8] {'kv'}, use_global_device_ids=true, to_apply=%region_8.9 | all-reduce | flops 32 | bytes 256 | tf_op jit(solution)/shard_map/psum | solution.py:114
  157.2 3.8 %fusion.18 = f32[32,2048]{1,0:T(8,128)} fusion(bf16[1024,2048]{1,0:T(8,128)(2,1)} %param.28, bf16[32,1024]{1,0:T(8,128)(2,1)S(1)} %get-tuple-element.205, f32[1024]{0:T(1024)S(1)} %dynamic_slice.59, f32[32]{0:T(128)S(1)} %add_rsqrt_fusion), kind=kOutput, calls=%fused_computation.37 | convolution fusion | flops 134348800 | bytes 4526208 | tf_op jit(solution)/shard_map/dot_general | solution.py:125
  161.1 23.8 %all-gather.8.cloned.1.call-done = f32[128,2048]{1,0:T(8,128)} async-done(((f32[32,2048]{1,0:T(8,128)}), f32[128,2048]{1,0:T(8,128)}) %all-gather.8.cloned.1.call-update) | async-done | bytes 1048592 | tf_op jit(solution)/shard_map/all_gather | solution.py:8
  184.9 1.3 reduce_sum.49
  186.3 3.7 %fusion.16 = f32[32,1024]{1,0:T(8,128)} fusion(bf16[2048,1024]{1,0:T(8,128)(2,1)} %param.29, f32[32,2048]{1,0:T(8,128)S(1)} %reduce_sum.49), kind=kOutput, calls=%fused_computation.34 | convolution fusion | flops 134414336 | bytes 4587520 | tf_op jit(solution)/shard_map/dot_general | solution.py:127
  189.9 30.7 %reduce-scatter.2.cloned.1.call-done = f32[32,128]{1,0:T(8,128)} async-done(((f32[32,1024]{1,0:T(8,128)}), f32[32,128]{1,0:T(8,128)}) %reduce-scatter.2.cloned.1.call-update) | async-done | bytes 16400 | tf_op jit(solution)/shard_map/reduce_scatter | solution.py:128
  220.7 1.3 add_convert_fusion.1
  (22 shorter events, 0.3 us)
Async XLA Ops:
  6.5 44.8 %copy-start = (bf16[4096,128]{1,0:T(8,128)(2,1)S(1)}, bf16[4096,128]{1,0:T(8,128)(2,1)}, u32[]{:S(2)}) copy-start(bf16[4096,128]{1,0:T(8,128)(2,1)} %param.18) | copy-start | bytes 3145732
  6.5 139.8 %all-reduce.2.cloned.1.call-start = ((), (), s32[]{:S(2)}) async-start(), calls=%async_computation.1 | async-start | bytes 262144 | tf_op jit(solution)/shard_map/psum | solution.py:109
  54.4 7.6 %copy-start.1 = (f32[32,2,1024]{2,1,0:T(2,128)S(1)}, f32[32,2,1024]{2,1,0:T(2,128)}, u32[]{:S(2)}) copy-start(f32[32,2,1024]{2,1,0:T(2,128)} %param.25) | copy-start | bytes 786436
  62.0 31.1 %copy-start.2 = (bf16[128,1024]{1,0:T(8,128)(2,1)S(1)}, bf16[128,1024]{1,0:T(8,128)(2,1)}, u32[]{:S(2)}) copy-start(bf16[128,1024]{1,0:T(8,128)(2,1)} %param.26) | copy-start | bytes 786436
  94.0 91.0 %all-gather.8.cloned.1.call-start = ((), (), s32[]{:S(2)}) async-start(), calls=%async_computation.3 | async-start | bytes 1310720 | tf_op jit(solution)/shard_map/all_gather | solution.py:8
  161.1 59.6 %reduce-scatter.2.cloned.1.call-start = ((), (), s32[]{:S(2)}) async-start(), calls=%async_computation.2 | async-start | bytes 147456 | tf_op jit(solution)/shard_map/reduce_scatter | solution.py:128
Sparse Core Ops, SparseCore 0:
  94.1 52.2 all-reduce.1
  161.2 23.7 all-gather.7
  190.1 30.5 reduce-scatter.1
